TPU v7x, 32 devices: a whole 2x2x4 slice. The times are simulated.
32 devices in a mesh: sp: 16 (over z, y, x), tp: 2 (over core).
Axes of the slice: x: 2, y: 2, z: 4, core: 2. Of those that a mesh axis runs over, the one named last changes fastest.
Arguments:
- queries: bfloat16 [4096, 1024], P('sp', 'tp'), may hold values from -7 to 7
- keys: bfloat16 [4096, 256], P('sp', 'tp'), may hold values from -6 to 6
- values: bfloat16 [4096, 256], P('sp', 'tp'), may hold values from -6 to 6
- q_gain: float32 [64], replicated, may hold values from 0.5 to 5
- k_gain: float32 [64], replicated, may hold values from 0.5 to 5
- resid: bfloat16 [4096, 2048], P(('sp', 'tp')), may hold values from -6 to 6
- out_weight: bfloat16 [1024, 2048], P('tp'), may hold values from -0.1875 to 0.1875
- post_gain: float32 [2048], replicated, may hold values from 0.1 to 1.9
- ffn_gain: float32 [2048], replicated, may hold values from 0.1 to 1.9
- post_ffn_gain: float32 [2048], replicated, may hold values from 0.1 to 1.9
- gate_w: bfloat16 [16, 2048, 3584], P('sp', None, 'tp'), may hold values from -0.125 to 0.125
- up_w: bfloat16 [16, 2048, 3584], P('sp', None, 'tp'), may hold values from -0.125 to 0.125
- down_w: bfloat16 [16, 3584, 2048], P('sp', 'tp'), may hold values from -0.09375 to 0.09375
- route_ids: int32 [4096, 2], P(('sp', 'tp')), may hold values from 0 to 15, all different within a row; in each aligned block of 128 rows (0 to 127, 128 to 255, ...) at most 24 rows name the same one
- route_w: float32 [4096, 2], P(('sp', 'tp')), may hold values from 0.2 to 1
Outputs:
- layer_out: bfloat16 [4096, 2048], P(('sp', 'tp'))
Inputs may be any that keep to these rules, and one draw needn't show every extreme that they name: `route_ids`: each row names 2 different experts. In each aligned block of 128 rows (the rows of one device) no expert is named more than 24 times, a bound that some blocks reach.
All inputs are finite; a program needn't handle non-finite values.
Results may differ from a plain program's by a relative error of at most 0.017.
The roundings to bfloat16 on the way count: a program that leaves them out, or rounds other values in their place, can miss the bound.
Values may be sent and summed in bfloat16 or wider, within the bound.
A program may use at most 128 MiB of HBM per device.

v0:
```python
import jax
import jax.numpy as jnp
from jax import lax
from jax.sharding import PartitionSpec as P

HEAD_DIM = 64
GRID_W = 64


EPS = 1e-06
THETA = 10000.0


def qk_prepare(raw, gain, positions, head_count):
    count_rows = raw.shape[0]
    values32 = raw.astype(jnp.float32).reshape(count_rows, head_count, HEAD_DIM)
    normed = (
        values32 * lax.rsqrt(jnp.mean(values32 * values32, axis=-1, keepdims=True) + EPS) * gain
    )
    half_dim = HEAD_DIM // 2
    freqs = THETA ** (-jnp.arange(0, half_dim, 2, dtype=jnp.float32) / half_dim)
    grid_row = (positions // GRID_W).astype(jnp.float32)
    grid_col = (positions % GRID_W).astype(jnp.float32)
    angles = jnp.concatenate([grid_row[:, None] * freqs, grid_col[:, None] * freqs], axis=-1)
    cosine = jnp.cos(angles)[:, None, :]
    sine = jnp.sin(angles)[:, None, :]
    paired = normed.reshape(count_rows, head_count, half_dim, 2)
    first = paired[..., 0]
    second = paired[..., 1]
    turned = jnp.stack([first * cosine - second * sine, first * sine + second * cosine], axis=-1)
    return turned.reshape(count_rows, head_count * HEAD_DIM).astype(jnp.bfloat16)


def rms_scale(values32, gain):
    return values32 * lax.rsqrt(jnp.mean(values32 * values32, axis=-1, keepdims=True) + EPS) * gain


def per_device(
    queries,
    keys,
    values,
    q_gain,
    k_gain,
    resid,
    out_weight,
    post_gain,
    ffn_gain,
    post_ffn_gain,
    gate_w,
    up_w,
    down_w,
    route_ids,
    route_w,
):
    tok_local = queries.shape[0]
    width = resid.shape[1]
    tp_count = lax.axis_size("tp")
    sp_count = lax.axis_size("sp")
    positions = lax.axis_index("sp") * tok_local + jnp.arange(tok_local, dtype=jnp.int32)
    head_local = queries.shape[1] // HEAD_DIM
    kv_local = keys.shape[1] // HEAD_DIM
    group_size = head_local // kv_local
    scale_factor = HEAD_DIM ** (-0.5)
    query_n = qk_prepare(queries, q_gain, positions, head_local).reshape(
        tok_local, kv_local, group_size, HEAD_DIM
    )
    key_n = qk_prepare(keys, k_gain, positions, kv_local)

    def key_step(carry, block):
        run_max, run_total, run_acc = carry
        block_keys, block_values = block
        scores = (
            jnp.einsum("qhgd,khd->hgqk", query_n, block_keys, preferred_element_type=jnp.float32)
            * scale_factor
        )
        new_max = jnp.maximum(run_max, jnp.max(scores, axis=-1))
        shrink_factor = jnp.exp(run_max - new_max)
        expo = jnp.exp(scores - new_max[..., None])
        run_total = run_total * shrink_factor + jnp.sum(expo, axis=-1)
        added = jnp.einsum(
            "hgqk,khd->hgqd",
            expo.astype(jnp.bfloat16),
            block_values,
            preferred_element_type=jnp.float32,
        )
        run_acc = run_acc * shrink_factor[..., None] + added
        return ((new_max, run_total, run_acc), None)

    initial = (
        jnp.full((kv_local, group_size, tok_local), -1e30, jnp.float32),
        jnp.zeros((kv_local, group_size, tok_local), jnp.float32),
        jnp.zeros((kv_local, group_size, tok_local, HEAD_DIM), jnp.float32),
    )
    carry = initial
    piece_keys = lax.all_gather(key_n, "sp", axis=0, tiled=True)
    piece_values = lax.all_gather(values, "sp", axis=0, tiled=True)
    length = piece_keys.shape[0]
    block_len = 512
    stacked_keys = piece_keys.reshape(length // block_len, block_len, kv_local, HEAD_DIM)
    stacked_values = piece_values.reshape(length // block_len, block_len, kv_local, HEAD_DIM)
    carry, unused = lax.scan(key_step, carry, (stacked_keys, stacked_values))
    run_max, run_total, run_acc = carry
    attended = jnp.transpose(run_acc / run_total[..., None], (2, 0, 1, 3))
    attended = attended.reshape(tok_local, head_local * HEAD_DIM).astype(jnp.bfloat16)
    row_count = tok_local // tp_count
    token_heads = lax.all_to_all(attended, "tp", split_axis=0, concat_axis=1, tiled=True)
    mixed = jnp.dot(
        token_heads,
        lax.all_gather(out_weight, "tp", axis=0, tiled=True),
        preferred_element_type=jnp.float32,
    )
    hidden_state = (resid.astype(jnp.float32) + rms_scale(mixed, post_gain)).astype(jnp.bfloat16)
    normed = rms_scale(hidden_state.astype(jnp.float32), ffn_gain).astype(jnp.bfloat16)
    top_count = route_ids.shape[1]
    expert_count = gate_w.shape[0] * sp_count
    capacity = 3 * tok_local * top_count // (2 * tp_count * expert_count)
    flat_routes = route_ids.reshape(-1)
    chosen = (flat_routes[:, None] == jnp.arange(expert_count, dtype=jnp.int32)[None, :]).astype(
        jnp.int32
    )
    earlier = jnp.cumsum(chosen, axis=0) - chosen
    ranks = jnp.sum(earlier * chosen, axis=1)
    slot_ids = flat_routes * capacity + ranks
    slot_range = jnp.arange(expert_count * capacity, dtype=jnp.int32)
    selector = jnp.sum(
        (slot_ids.reshape(row_count, top_count)[:, :, None] == slot_range[None, None, :]).astype(
            jnp.bfloat16
        ),
        axis=1,
    )
    outgoing = lax.dot_general(
        selector, normed, (((0,), (0,)), ((), ())), preferred_element_type=jnp.float32
    )
    outgoing = outgoing.astype(jnp.bfloat16).reshape(expert_count, capacity, width)
    arrived = lax.all_to_all(outgoing, "sp", split_axis=0, concat_axis=0, tiled=True)
    flat_rows = lax.all_gather(arrived, "tp", axis=0, tiled=True).reshape(-1, width)
    gate = jnp.dot(flat_rows, gate_w[0], preferred_element_type=jnp.float32)
    upward = jnp.dot(flat_rows, up_w[0], preferred_element_type=jnp.float32)
    inner = (jax.nn.silu(gate) * upward).astype(jnp.bfloat16)
    expert_out = lax.psum_scatter(
        jnp.dot(inner, down_w[0], preferred_element_type=jnp.float32).astype(jnp.bfloat16),
        "tp",
        scatter_dimension=0,
        tiled=True,
    )
    returned = lax.all_to_all(
        expert_out.reshape(expert_count, capacity, width),
        "sp",
        split_axis=0,
        concat_axis=0,
        tiled=True,
    )
    picked = returned.reshape(expert_count * capacity, width)[slot_ids]
    picked = picked.reshape(row_count, top_count, width).astype(jnp.float32)
    combined = jnp.sum(route_w[:, :, None] * picked, axis=1)
    return (hidden_state.astype(jnp.float32) + rms_scale(combined, post_ffn_gain)).astype(
        jnp.bfloat16
    )


def solution(mesh):
    in_specs = (
        P("sp", "tp"),
        P("sp", "tp"),
        P("sp", "tp"),
        P(),
        P(),
        P(("sp", "tp"), None),
        P("tp", None),
        P(),
        P(),
        P(),
        P("sp", None, "tp"),
        P("sp", None, "tp"),
        P("sp", "tp", None),
        P(("sp", "tp"), None),
        P(("sp", "tp"), None),
    )
    out_specs = P(("sp", "tp"), None)
    return jax.shard_map(
        per_device, mesh=mesh, in_specs=in_specs, out_specs=out_specs, check_vma=False
    )
```

profile of v0, /device:TPU:0, one launch (start us, length us, event | category | flops | bytes accessed | tf_op | source)
XLA Modules:
  0.0 367.1 jit_solution(12155607543420647060)
XLA Ops:
  16.3 51.5 %all-gather.5.cloned.1.call-done = bf16[4096,128]{0,1:T(8,128)(2,1)} async-done(((bf16[256,128]{0,1:T(8,128)(2,1)}), bf16[4096,128]{0,1:T(8,128)(2,1)}) %all-gather.5.cloned.1.call-update) | async-done | bytes 1048592 | tf_op jit(solution)/shard_map/all_gather | solution.py:95
  70.8 53.6 %all-gather.7.cloned.1.call-done = bf16[4096,128]{1,0:T(8,128)(2,1)} async-done(((bf16[256,128]{1,0:T(8,128)(2,1)}), bf16[4096,128]{1,0:T(8,128)(2,1)}) %all-gather.7.cloned.1.call-update) | async-done | bytes 1048592 | tf_op jit(solution)/shard_map/all_gather | solution.py:96
  124.4 3.9 %reshape.265 = bf16[8,512,2,64]{3,2,1,0:T(2,128)(2,1)S(1)} reshape(bf16[4096,128]{1,0:T(8,128)(2,1)} %all-gather.7.cloned.1.call-done) | data formatting | bytes 2097152 | tf_op jit(solution)/shard_map/reshape | solution.py:100
  128.2 3.5 copy.62
  131.7 72.0 %while.15 = (s32[]{:T(128)}, f32[2,4,256]{2,1,0:T(4,128)S(1)}, f32[2,4,256]{2,1,0:T(4,128)S(1)}, f32[2,4,256,64]{2,3,1,0:T(8,128)S(1)}, bf16[8,512,2,64]{1,3,2,0...) while((s32[]{:T(128)}, f32[2,4,256]{2,1,0:T(4,128)S(1)}, ...), condition=%wide.region_5.6_spmd.clone, body=%wide.region_2.5_spmd.clone.sunk | while | flops 277227520 | bytes 31065220 | solution.py:101
  131.7 3.8 %bitcast_reduce_fusion.4 = (f32[2,4,256]{2,1,0:T(4,128)S(1)}, f32[2,512,256,4]{2,1,3,0:T(8,128)}) fusion(bf16[256,2,4,64]{0,3,2,1:T(8,128)(2,1)S(1)} %get-tuple-element.205, bf16[8,512,2,64]{1,3,2,0:T(8,128)(2,1)} %get-tuple-element.204, s32[]{:T(128)} %get-tuple-element.191), kind=kOutput, calls=%fused_computation.2.clone.1 | convolution fusion | flops 136312832 | bytes 4596224 | tf_op jit(solution)/shard_map/while/body/eval_jaxpr/qhgd,khd->hgqk/dot_general | solution.py:73
  135.5 3.2 fusion.71
  141.0 3.6 bitcast_reduce_fusion.4
  144.7 3.0 fusion.71
  150.0 3.6 bitcast_reduce_fusion.4
  159.0 3.6 bitcast_reduce_fusion.4
  167.9 3.6 bitcast_reduce_fusion.4
  176.9 3.6 bitcast_reduce_fusion.4
  185.8 3.6 bitcast_reduce_fusion.4
  194.8 3.6 bitcast_reduce_fusion.4
  204.0 3.9 %all_to_all.26 = bf16[2,128,512]{1,2,0:T(8,128)(2,1)S(1)} all-to-all(bf16[2,128,512]{1,2,0:T(8,128)(2,1)S(1)} %copy.63), channel_id=1, replica_groups=mesh['sp'=16,'tp'=2] {'tp'}, dimensions={0} | all-to-all | bytes 524288 | tf_op jit(solution)/shard_map/all_to_all | solution.py:106
  212.0 43.0 %all_to_all.27 = bf16[16,24,2048]{2,1,0:T(8,128)(2,1)} all-to-all(bf16[16,24,2048]{2,1,0:T(8,128)(2,1)S(1)} %bitcast.113), channel_id=1, replica_groups=mesh['sp'=16,'tp'=2] {'sp'}, dimensions={0} | all-to-all | bytes 3145728 | tf_op jit(solution)/shard_map/all_to_all | solution.py:135
  255.3 10.4 %all-gather.11.cloned.1.call-done = bf16[32,24,2048]{2,1,0:T(8,128)(2,1)} async-done(((bf16[16,24,2048]{2,1,0:T(8,128)(2,1)}), bf16[32,24,2048]{2,1,0:T(8,128)(2,1)}) %all-gather.11.cloned.1.call-update) | async-done | bytes 3145744 | tf_op jit(solution)/shard_map/all_gather | solution.py:136
  265.6 11.1 %fusion.23 = f32[768,1792]{1,0:T(8,128)} fusion(bf16[768,2048]{1,0:T(8,128)(2,1)} %bitcast.120, bf16[1,2048,1792]{2,1,0:T(8,128)(2,1)} %param.27), kind=kOutput, calls=%fused_computation.27 | convolution fusion | flops 5637144576 | bytes 15990784 | tf_op jit(solution)/shard_map/dot_general | solution.py:137
  276.8 21.0 %fusion.29 = bf16[768,2048]{1,0:T(8,128)(2,1)} fusion(bf16[1,1792,2048]{2,1,0:T(8,128)(2,1)} %param.29, f32[768,1792]{1,0:T(8,128)} %fusion.23, bf16[768,2048]{1,0:T(8,128)(2,1)} %bitcast.121, bf16[1,2048,1792]{2,1,0:T(8,128)(2,1)} %param.28), kind=kOutput, calls=%fused_computation.30 | convolution fusion | flops 11284119552 | bytes 26476544 | tf_op jit(solution)/shard_map/dot_general | solution.py:141
  297.9 12.5 %reduce-scatter.2.cloned.1.call-done = bf16[384,2048]{1,0:T(8,128)(2,1)} async-done(((bf16[768,2048]{1,0:T(8,128)(2,1)}), bf16[384,2048]{1,0:T(8,128)(2,1)}) %reduce-scatter.2.cloned.1.call-update) | async-done | bytes 1572880 | tf_op jit(solution)/shard_map/reduce_scatter | solution.py:140
  310.4 6.9 %all-to-all-start.2 = ((bf16[16,24,2048]{2,1,0:T(8,128)(2,1)}), bf16[16,24,2048]{2,1,0:T(8,128)(2,1)S(1)}, u32[]{:S(2)}, u32[]{:S(2)}) async-start(bf16[16,24,2048]{2,1,0:T(8,128)(2,1)} %bitcast.115), calls=%async_computation.3 | async-start | bytes 3145728 | tf_op jit(solution)/shard_map/all_to_all | solution.py:146
  317.5 33.9 %all-to-all-done.2 = bf16[16,24,2048]{2,1,0:T(8,128)(2,1)S(1)} async-done(((bf16[16,24,2048]{2,1,0:T(8,128)(2,1)}), bf16[16,24,2048]{2,1,0:T(8,128)(2,1)S(1)}, u32[]{:S(2)}, u32[]{:S(2)}) %all-to-all-start.2) | async-done | bytes 1572896 | tf_op jit(solution)/shard_map/all_to_all | solution.py:146
  356.2 3.2 multiply_reduce_fusion
  (136 shorter events, 59.5 us)
Async XLA Ops:
  6.5 6.2 %copy-start.5 = (s32[128,2]{0,1:T(2,128)S(1)}, s32[128,2]{0,1:T(2,128)}, u32[]{:S(2)}) copy-start(s32[128,2]{0,1:T(2,128)} %param.30) | copy-start | bytes 3076
  6.5 6.6 %copy-start.7 = (f32[64]{0:T(128)S(1)}, f32[64]{0:T(128)}, u32[]{:S(2)}) copy-start(f32[64]{0:T(128)} %param.20) | copy-start | bytes 772
  6.5 61.3 %all-gather.5.cloned.1.call-start = ((), (), s32[]{:S(2)}) async-start(), calls=%async_computation.4 | async-start | bytes 1114112 | tf_op jit(solution)/shard_map/all_gather | solution.py:95
  9.8 114.6 %all-gather.7.cloned.1.call-start = ((), (), s32[]{:S(2)}) async-start(), calls=%async_computation.5 | async-start | bytes 1114112 | tf_op jit(solution)/shard_map/all_gather | solution.py:96
  10.5 197.4 %all-gather.9.cloned.1.call-start = ((), (), s32[]{:S(2)}) async-start(), calls=%async_computation.6 | async-start | bytes 6291456 | tf_op jit(solution)/shard_map/all_gather | solution.py:109
  11.3 254.4 %all-gather.11.cloned.1.call-start = ((), (), s32[]{:S(2)}) async-start(), calls=%async_computation.7 | async-start | bytes 4718592 | tf_op jit(solution)/shard_map/all_gather | solution.py:136
  135.5 3.7 copy-start
  144.7 3.4 copy-start
  153.6 3.4 copy-start
  162.6 3.4 copy-start
  171.5 3.4 copy-start
  180.5 3.4 copy-start
  189.5 3.4 copy-start
  198.4 3.4 copy-start
  203.8 7.2 %copy-start.1 = (bf16[128,2048]{1,0:T(8,128)(2,1)S(1)}, bf16[128,2048]{1,0:T(8,128)(2,1)}, u32[]{:S(2)}) copy-start(bf16[128,2048]{1,0:T(8,128)(2,1)} %param.22) | copy-start | bytes 1572868
  203.8 7.2 %copy-start.2 = (f32[2048]{0:T(1024)S(1)}, f32[2048]{0:T(1024)}, u32[]{:S(2)}) copy-start(f32[2048]{0:T(1024)} %param.24) | copy-start | bytes 24580
  204.0 7.4 %copy-start.3 = (f32[2048]{0:T(1024)S(1)}, f32[2048]{0:T(1024)}, u32[]{:S(2)}) copy-start(f32[2048]{0:T(1024)} %param.25) | copy-start | bytes 24580
  255.0 55.3 %reduce-scatter.2.cloned.1.call-start = ((), (), s32[]{:S(2)}) async-start(), calls=%async_computation.8 | async-start | bytes 4718592 | tf_op jit(solution)/shard_map/reduce_scatter | solution.py:140
  297.8 19.6 %copy-start.6 = (f32[128,2]{0,1:T(2,128)S(1)}, f32[128,2]{0,1:T(2,128)}, u32[]{:S(2)}) copy-start(f32[128,2]{0,1:T(2,128)} %param.31) | copy-start | bytes 3076
  310.4 41.1 %all-to-all-start.2 = ((bf16[16,24,2048]{2,1,0:T(8,128)(2,1)}), bf16[16,24,2048]{2,1,0:T(8,128)(2,1)S(1)}, u32[]{:S(2)}, u32[]{:S(2)}) async-start(bf16[16,24,2048]{2,1,0:T(8,128)(2,1)} %bitcast.115), calls=%async_computation.3 | async-start | bytes 3145728 | tf_op jit(solution)/shard_map/all_to_all | solution.py:146
  353.8 5.7 %copy-start.4 = (f32[2048]{0:T(1024)S(1)}, f32[2048]{0:T(1024)}, u32[]{:S(2)}) copy-start(f32[2048]{0:T(1024)} %param.26) | copy-start | bytes 24580
Sparse Core Ops, SparseCore 0:
  10.1 57.6 all-gather.4
  70.6 53.7 all-gather.6
  125.9 12.4 all-gather.8
  255.2 10.4 all-gather.10
  298.0 12.3 reduce-scatter.1
where the time goes:
time: 370 us; the launch traced here: 367 us
  waiting for transfers between devices  163 us (44%)
  matrix products  79.8 us (22%)
  blocking collectives  46.9 us (13%)
  other arithmetic  32.8 us (9%)
  local copies, waits for them, and re-layouts  23.2 us (6%)
  between operations  13.5 us (4%)
  starting transfers between devices  7.23 us (2%)
    all_gather x1, waiting for transfers between devices, per_device(): piece_values = lax.all_gather(values, 'sp', axis=0, tiled=True)  53.6 us
    all_gather x1, waiting for transfers between devices, per_device(): piece_keys = lax.all_gather(key_n, 'sp', axis=0, tiled=True)  51.5 us
    all_to_all x1, blocking collectives, per_device(): lax.all_to_all(outgoing, 'sp', split_axis=0, concat_axis=0, tiled=True)  43 us
    all_to_all x1, waiting for transfers between devices, per_device(): lax.all_to_all(expert_out.reshape(expert_count, capacity, width), 'sp', s...  33.9 us
    dot_general x8, matrix products, key_step(): jnp.einsum('qhgd,khd->hgqk', query_n, block_keys, preferred_element_type=...  29.2 us
    reduce_sum x8, other arithmetic, key_step(): run_total = run_total * shrink_factor + jnp.sum(expo, axis=-1)  24.5 us
    dot_general x1, matrix products, per_device(): jnp.dot(inner, down_w[0], preferred_element_type=jnp.float32)  21 us
    dot_general x8, matrix products, key_step(): jnp.einsum('hgqk,khd->hgqd', expo.astype(jnp.bfloat16), block_values, pre...  14.8 us
  transfers between devices with their start and end apart: 6, of which 5 were waited for; matrix products, arithmetic and copies ran while one was open for 23% of the time, Pallas kernels for 0%

commit v1 on v0

v1 whole, which is shorter than its diff:
```python
import functools

import jax
import jax.numpy as jnp
from jax import lax
from jax.experimental import pallas as pl
from jax.experimental.pallas import tpu as pltpu
from jax.sharding import PartitionSpec as P

HEAD_DIM = 64
GRID_W = 64


EPS = 1e-06
THETA = 10000.0


LANES = 128
EXP2_SCALE = HEAD_DIM ** (-0.5) * 1.4426950408889634
MESH = pl.DeviceIdType.MESH


def turn_tables(positions):
    lane = jnp.arange(LANES, dtype=jnp.int32) % HEAD_DIM
    pair = lane // 2
    quarter = HEAD_DIM // 4
    freqs = THETA ** (-2.0 * (pair % quarter).astype(jnp.float32) / (HEAD_DIM // 2))
    grid_row = (positions // GRID_W).astype(jnp.float32)[:, None]
    grid_col = (positions % GRID_W).astype(jnp.float32)[:, None]
    angles = jnp.where(pair < quarter, grid_row, grid_col) * freqs
    sign = jnp.where(lane % 2 == 0, -1.0, 1.0)
    return jnp.cos(angles), jnp.sin(angles) * sign


def prep_kernel(q_ref, k_ref, v_ref, gains_ref, cos_ref, sin_ref, qz_ref, pay_ref):
    tok = q_ref.shape[0]
    heads = q_ref.shape[1] // HEAD_DIM
    group = heads // (k_ref.shape[1] // HEAD_DIM)
    row = lax.broadcasted_iota(jnp.int32, (LANES, LANES), 0) // HEAD_DIM
    col = lax.broadcasted_iota(jnp.int32, (LANES, LANES), 1) // HEAD_DIM
    mean_mat = jnp.where(row == col, 1.0 / HEAD_DIM, 0.0).astype(jnp.float32)
    even = lax.broadcasted_iota(jnp.int32, (tok, LANES), 1) % 2 == 0
    cosine = cos_ref[...]
    sine = sin_ref[...]

    def turned(raw, gain):
        x = raw.astype(jnp.float32)
        mean = jnp.dot(
            x * x, mean_mat, precision=lax.Precision.HIGHEST, preferred_element_type=jnp.float32
        )
        normed = x * lax.rsqrt(mean + EPS) * gain
        swapped = jnp.where(even, pltpu.roll(normed, LANES - 1, 1), pltpu.roll(normed, 1, 1))
        return normed * cosine + swapped * sine

    qz_ref[...] = jnp.zeros(qz_ref.shape, qz_ref.dtype)
    for tile in range(q_ref.shape[1] // LANES):
        out = turned(q_ref[:, tile * LANES : (tile + 1) * LANES], gains_ref[0:1, :])
        flipped = out.T.astype(jnp.bfloat16)
        for part in range(LANES // HEAD_DIM):
            head = tile * (LANES // HEAD_DIM) + part
            base = (head // group) * HEAD_DIM
            qz_ref[head, base : base + HEAD_DIM, :] = flipped[
                part * HEAD_DIM : (part + 1) * HEAD_DIM
            ]
    pay_ref[0:tok, :] = turned(k_ref[...], gains_ref[1:2, :]).astype(jnp.bfloat16)
    for tile in range(tok // LANES):
        block = v_ref[tile * LANES : (tile + 1) * LANES, :].astype(jnp.float32)
        pay_ref[tok + tile * LANES : tok + (tile + 1) * LANES, :] = block.T.astype(jnp.bfloat16)


def attend_kernel(
    count, group, qz_ref, pay_ref, out_ref, held, run_max, run_sum, run_acc, send_sem, recv_sem
):
    me = lax.axis_index("sp")
    heads = qz_ref.shape[0]
    tok = qz_ref.shape[2]

    barrier = pltpu.get_barrier_semaphore()
    for step in range(1, count):
        pl.semaphore_signal(
            barrier, inc=1, device_id={"sp": lax.rem(me + step, count)}, device_id_type=MESH
        )
    pl.semaphore_wait(barrier, count - 1)

    def send(step):
        return pltpu.make_async_remote_copy(
            src_ref=pay_ref,
            dst_ref=held.at[me],
            send_sem=send_sem.at[step],
            recv_sem=recv_sem.at[me],
            device_id={"sp": lax.rem(me + step, count)},
            device_id_type=MESH,
        )

    for step in range(1, count):
        send(step).start()

    def block(keys, values_t, first):
        for head in range(heads):
            base = (head // group) * HEAD_DIM
            rows = pl.ds(head * HEAD_DIM, HEAD_DIM)
            one = pl.ds(head, 1)
            scores = jnp.dot(keys, qz_ref[head], preferred_element_type=jnp.float32)
            top = jnp.max(scores, axis=0, keepdims=True)
            if not first:
                old = run_max[one, :]
                top = jnp.maximum(old, top)
            expo = jnp.exp2((scores - top) * EXP2_SCALE)
            total = jnp.sum(expo, axis=0, keepdims=True)
            added = jnp.dot(
                values_t[base : base + HEAD_DIM],
                expo.astype(jnp.bfloat16),
                preferred_element_type=jnp.float32,
            )
            if not first:
                shrink = jnp.exp2((old - top) * EXP2_SCALE)
                total = total + run_sum[one, :] * shrink
                added = added + run_acc[rows, :] * shrink
            run_max[one, :] = top
            run_sum[one, :] = total
            run_acc[rows, :] = added

    def split(ref):
        tiles = [ref[tok + t * LANES : tok + (t + 1) * LANES, :] for t in range(tok // LANES)]
        return ref[0:tok, :], jnp.concatenate(tiles, axis=1)

    block(*split(pay_ref), True)

    @pl.loop(1, count)
    def _(step):
        owner = lax.rem(me - step + count, count)
        pltpu.make_async_copy(held.at[owner], held.at[owner], recv_sem.at[owner]).wait()
        block(*split(held.at[owner]), False)

    for head in range(0, heads, LANES // HEAD_DIM):
        parts = []
        for h in range(head, head + LANES // HEAD_DIM):
            rows = pl.ds(h * HEAD_DIM, HEAD_DIM)
            parts.append(run_acc[rows, :] / run_sum[pl.ds(h, 1), :])
        both = jnp.concatenate(parts, axis=0)
        out_ref[:, head * HEAD_DIM : head * HEAD_DIM + LANES] = both.T.astype(jnp.bfloat16)
    for step in range(1, count):
        send(step).wait_send()


def attention(queries, keys, values, q_gain, k_gain):
    tok = queries.shape[0]
    sp_count = lax.axis_size("sp")
    heads = queries.shape[1] // HEAD_DIM
    kv_heads = keys.shape[1] // HEAD_DIM
    positions = lax.axis_index("sp") * tok + jnp.arange(tok, dtype=jnp.int32)
    cosine, sine = turn_tables(positions)
    gains = jnp.tile(jnp.stack([q_gain, k_gain]), (1, LANES // HEAD_DIM))
    vmem = pl.BlockSpec(memory_space=pltpu.VMEM)
    qz, payload = pl.pallas_call(
        prep_kernel,
        out_shape=(
            jax.ShapeDtypeStruct((heads, LANES, tok), jnp.bfloat16),
            jax.ShapeDtypeStruct((2 * tok, LANES), jnp.bfloat16),
        ),
        in_specs=[vmem] * 6,
        out_specs=(vmem, vmem),
        name="prep",
    )(queries, keys, values, gains, cosine, sine)
    return pl.pallas_call(
        functools.partial(attend_kernel, sp_count, heads // kv_heads),
        out_shape=jax.ShapeDtypeStruct((tok, heads * HEAD_DIM), jnp.bfloat16),
        in_specs=[vmem] * 2,
        out_specs=vmem,
        scratch_shapes=[
            pltpu.VMEM((sp_count, 2 * tok, LANES), jnp.bfloat16),
            pltpu.VMEM((heads, tok), jnp.float32),
            pltpu.VMEM((heads, tok), jnp.float32),
            pltpu.VMEM((heads * HEAD_DIM, tok), jnp.float32),
            pltpu.SemaphoreType.DMA((sp_count,)),
            pltpu.SemaphoreType.DMA((sp_count,)),
        ],
        compiler_params=pltpu.CompilerParams(collective_id=0, has_side_effects=True),
        cost_estimate=pl.CostEstimate(
            flops=4 * sp_count * tok * tok * heads * HEAD_DIM,
            bytes_accessed=4 * sp_count * tok * LANES,
            transcendentals=sp_count * tok * tok * heads,
        ),
        name="attend",
    )(qz, payload)


def rms_scale(values32, gain):
    return values32 * lax.rsqrt(jnp.mean(values32 * values32, axis=-1, keepdims=True) + EPS) * gain


def per_device(
    queries,
    keys,
    values,
    q_gain,
    k_gain,
    resid,
    out_weight,
    post_gain,
    ffn_gain,
    post_ffn_gain,
    gate_w,
    up_w,
    down_w,
    route_ids,
    route_w,
):
    tok_local = queries.shape[0]
    width = resid.shape[1]
    tp_count = lax.axis_size("tp")
    sp_count = lax.axis_size("sp")
    attended = attention(queries, keys, values, q_gain, k_gain)
    row_count = tok_local // tp_count
    token_heads = lax.all_to_all(attended, "tp", split_axis=0, concat_axis=1, tiled=True)
    mixed = jnp.dot(
        token_heads,
        lax.all_gather(out_weight, "tp", axis=0, tiled=True),
        preferred_element_type=jnp.float32,
    )
    hidden_state = (resid.astype(jnp.float32) + rms_scale(mixed, post_gain)).astype(jnp.bfloat16)
    normed = rms_scale(hidden_state.astype(jnp.float32), ffn_gain).astype(jnp.bfloat16)
    top_count = route_ids.shape[1]
    expert_count = gate_w.shape[0] * sp_count
    capacity = 3 * tok_local * top_count // (2 * tp_count * expert_count)
    flat_routes = route_ids.reshape(-1)
    chosen = (flat_routes[:, None] == jnp.arange(expert_count, dtype=jnp.int32)[None, :]).astype(
        jnp.int32
    )
    earlier = jnp.cumsum(chosen, axis=0) - chosen
    ranks = jnp.sum(earlier * chosen, axis=1)
    slot_ids = flat_routes * capacity + ranks
    slot_range = jnp.arange(expert_count * capacity, dtype=jnp.int32)
    selector = jnp.sum(
        (slot_ids.reshape(row_count, top_count)[:, :, None] == slot_range[None, None, :]).astype(
            jnp.bfloat16
        ),
        axis=1,
    )
    outgoing = lax.dot_general(
        selector, normed, (((0,), (0,)), ((), ())), preferred_element_type=jnp.float32
    )
    outgoing = outgoing.astype(jnp.bfloat16).reshape(expert_count, capacity, width)
    arrived = lax.all_to_all(outgoing, "sp", split_axis=0, concat_axis=0, tiled=True)
    flat_rows = lax.all_gather(arrived, "tp", axis=0, tiled=True).reshape(-1, width)
    gate = jnp.dot(flat_rows, gate_w[0], preferred_element_type=jnp.float32)
    upward = jnp.dot(flat_rows, up_w[0], preferred_element_type=jnp.float32)
    inner = (jax.nn.silu(gate) * upward).astype(jnp.bfloat16)
    expert_out = lax.psum_scatter(
        jnp.dot(inner, down_w[0], preferred_element_type=jnp.float32).astype(jnp.bfloat16),
        "tp",
        scatter_dimension=0,
        tiled=True,
    )
    returned = lax.all_to_all(
        expert_out.reshape(expert_count, capacity, width),
        "sp",
        split_axis=0,
        concat_axis=0,
        tiled=True,
    )
    picked = returned.reshape(expert_count * capacity, width)[slot_ids]
    picked = picked.reshape(row_count, top_count, width).astype(jnp.float32)
    combined = jnp.sum(route_w[:, :, None] * picked, axis=1)
    return (hidden_state.astype(jnp.float32) + rms_scale(combined, post_ffn_gain)).astype(
        jnp.bfloat16
    )


def solution(mesh):
    in_specs = (
        P("sp", "tp"),
        P("sp", "tp"),
        P("sp", "tp"),
        P(),
        P(),
        P(("sp", "tp"), None),
        P("tp", None),
        P(),
        P(),
        P(),
        P("sp", None, "tp"),
        P("sp", None, "tp"),
        P("sp", "tp", None),
        P(("sp", "tp"), None),
        P(("sp", "tp"), None),
    )
    out_specs = P(("sp", "tp"), None)
    return jax.shard_map(
        per_device, mesh=mesh, in_specs=in_specs, out_specs=out_specs, check_vma=False
    )
```

time: 370 us -> 254 us (0.69)
  waiting for transfers between devices: 163 us -> 57.8 us
  Pallas kernels: 0 us -> 64.1 us
  matrix products: 79.8 us -> 35.9 us
  other arithmetic: 32.8 us -> 7.73 us
  local copies, waits for them, and re-layouts: 23.2 us -> 8.31 us
  blocking collectives: 46.9 us -> 53.9 us
    all_gather x2 -> x0, waiting for transfers between devices: 105 us -> none  [the longest x1 53.6 us: per_device(): piece_values = lax.all_gather(values, 'sp', axis=0, tiled=True)]
    pallas_call x0 -> x2, Pallas kernels: none -> 64.1 us  [the longest x1 61.1 us: attention(): pl.pallas_call(functools.partial(attend_kernel, sp_count, heads // kv_hea...]
    dot_general x16 -> x0, matrix products: 44 us -> none  [the longest x8 29.2 us: key_step(): jnp.einsum('qhgd,khd->hgqk', query_n, block_keys, preferred_element_type=...]
    reduce_sum x10 -> x0, other arithmetic: 24.6 us -> none  [the longest x8 24.5 us: key_step(): run_total = run_total * shrink_factor + jnp.sum(expo, axis=-1)]
    all_to_all x1, blocking collectives: 43 us -> 53.9 us  [per_device(): lax.all_to_all(outgoing, 'sp', split_axis=0, concat_axis=0, tiled=True)]
    unnamed x21 -> x14, local copies, waits for them, and re-layouts: 8.77 us -> 0.26 us
    reshape x3 -> x0, local copies, waits for them, and re-layouts: 4.19 us -> none  [the longest x1 3.87 us: per_device(): piece_values.reshape(length // block_len, block_len, kv_local, HEAD_DIM)]
    all_to_all x1 -> x0, blocking collectives: 3.94 us -> none  [per_device(): lax.all_to_all(attended, 'tp', split_axis=0, concat_axis=1, tiled=True)]
  transfers between devices with their start and end apart: 6 -> 5, of which waited for: 5 -> 3; matrix products, arithmetic and copies ran while one was open for 23% -> 3% of each run, Pallas kernels for 0% -> 25%
where the time goes in v1:
time: 254 us; the launch traced here: 252 us
  Pallas kernels  64.1 us (25%)
  waiting for transfers between devices  57.8 us (23%)
  blocking collectives  53.9 us (21%)
  matrix products  35.9 us (14%)
  between operations  13.3 us (5%)
  starting transfers between devices  10.6 us (4%)
  local copies, waits for them, and re-layouts  8.31 us (3%)
  other arithmetic  7.73 us (3%)
    pallas_call x1, Pallas kernels, attention(): pl.pallas_call(functools.partial(attend_kernel, sp_count, heads // kv_hea...  61.1 us
    all_to_all x1, blocking collectives, per_device(): lax.all_to_all(outgoing, 'sp', split_axis=0, concat_axis=0, tiled=True)  53.9 us
    all_to_all x1, waiting for transfers between devices, per_device(): lax.all_to_all(expert_out.reshape(expert_count, capacity, width), 'sp', s...  34 us
    dot_general x1, matrix products, per_device(): jnp.dot(inner, down_w[0], preferred_element_type=jnp.float32)  21 us
    reduce_scatter x1, waiting for transfers between devices, per_device(): lax.psum_scatter(jnp.dot(inner, down_w[0], preferred_element_type=jnp.flo...  12.5 us
    dot_general x1, matrix products, per_device(): gate = jnp.dot(flat_rows, gate_w[0], preferred_element_type=jnp.float32)  11.1 us
    all_gather x1, waiting for transfers between devices, per_device(): lax.all_gather(arrived, 'tp', axis=0, tiled=True).reshape(-1, width)  10.5 us
    all_to_all x1, starting transfers between devices, per_device(): lax.all_to_all(expert_out.reshape(expert_count, capacity, width), 'sp', s...  6.89 us
  transfers between devices with their start and end apart: 5, of which 3 were waited for; matrix products, arithmetic and copies ran while one was open for 3% of the time, Pallas kernels for 25%

profile of v1, /device:TPU:0, one launch (start us, length us, event | category | flops | bytes accessed | tf_op | source)
XLA Modules:
  0.0 251.5 jit_solution(7070853216729817356)
XLA Ops:
  6.5 0.7 all-gather.3.cloned.1.call-update
  7.3 0.7 pad_maximum_fusion
  7.9 0.7 tile.10.gains_ref
  8.7 1.2 sine_multiply_fusion
  9.9 2.9 %prep.1 = (bf16[8,128,256]{2,1,0:T(8,128)(2,1)}, bf16[512,128]{1,0:T(8,128)(2,1)}) custom-call(bf16[256,512]{1,0:T(8,128)(2,1)} %q_ref.1, bf16[256,128]{1,0:T(8,128)(2,1)} %k_ref.1, bf16[256,128]{1,0:T(8,128)(2,1)} %v_ref.1, f32[2,128]{1,0:T(2,128)} %tile.10.gains_ref, f32[256,128]{1,0:T(8,128)} %get-tuple-element.14.cos_ref, ...), custom_call_target="tpu_custom_call" | custom-call | tf_op jit(solution)/shard_map/prep/pallas_call | solution.py:155
  12.9 61.1 %attend.1 = bf16[256,512]{1,0:T(8,128)(2,1)} custom-call(bf16[8,128,256]{2,1,0:T(8,128)(2,1)} %get-tuple-element.7.qz_ref, bf16[512,128]{1,0:T(8,128)(2,1)} %get-tuple-element.8.pay_ref), custom_call_target="tpu_custom_call" | custom-call | flops 2147483648 | bytes 2097152 | tf_op jit(solution)/shard_map/attend/pallas_call | solution.py:165
  74.0 1.8 copy.30
  75.9 3.4 %all-to-all-start = ((bf16[2,128,512]{1,2,0:T(8,128)(2,1)}), bf16[2,128,512]{1,2,0:T(8,128)(2,1)S(1)}, u32[]{:S(2)}, u32[]{:S(2)}) async-start(bf16[2,128,512]{1,2,0:T(8,128)(2,1)} %copy.30), calls=%async_computation | async-start | bytes 524288 | tf_op jit(solution)/shard_map/all_to_all | solution.py:215
  79.8 0.6 reduce-window.6
  81.1 3.0 %multiply_reduce_fusion.2 = (f32[128]{0:T(128)S(1)}, f32[128,2048]{1,0:T(8,128)S(1)}) fusion(bf16[128,1024]{0,1:T(8,128)(2,1)S(1)} %bitcast.56, bf16[1024,2048]{1,0:T(8,128)(2,1)} %all-gather.3.cloned.1.call-done), kind=kOutput, calls=%fused_computation.21 | convolution fusion | flops 537395072 | bytes 5505536 | tf_op jit(solution)/shard_map/dot_general | solution.py:216
  84.2 0.4 fusion.16
  84.6 0.7 convolution_convert_fusion
  85.2 53.9 %all_to_all.29 = bf16[16,24,2048]{2,1,0:T(8,128)(2,1)} all-to-all(bf16[16,24,2048]{2,1,0:T(8,128)(2,1)S(1)} %bitcast.54), channel_id=1, replica_groups=mesh['sp'=16,'tp'=2] {'sp'}, dimensions={0} | all-to-all | bytes 3145728 | tf_op jit(solution)/shard_map/all_to_all | solution.py:244
  139.1 0.2 reduce-scatter.2.cloned.1.call-start
  139.4 10.5 %all-gather.5.cloned.1.call-done = bf16[32,24,2048]{2,1,0:T(8,128)(2,1)} async-done(((bf16[16,24,2048]{2,1,0:T(8,128)(2,1)}), bf16[32,24,2048]{2,1,0:T(8,128)(2,1)}) %all-gather.5.cloned.1.call-update) | async-done | bytes 3145744 | tf_op jit(solution)/shard_map/all_gather | solution.py:245
  149.9 11.1 %fusion.4 = f32[768,1792]{1,0:T(8,128)} fusion(bf16[768,2048]{1,0:T(8,128)(2,1)} %bitcast.62, bf16[1,2048,1792]{2,1,0:T(8,128)(2,1)} %param.25), kind=kOutput, calls=%fused_computation.5 | convolution fusion | flops 5637144576 | bytes 15990784 | tf_op jit(solution)/shard_map/dot_general | solution.py:246
  161.1 21.0 %fusion.10 = bf16[768,2048]{1,0:T(8,128)(2,1)} fusion(bf16[1,1792,2048]{2,1,0:T(8,128)(2,1)} %param.27, f32[768,1792]{1,0:T(8,128)} %fusion.4, bf16[768,2048]{1,0:T(8,128)(2,1)} %bitcast.63, bf16[1,2048,1792]{2,1,0:T(8,128)(2,1)} %param.26), kind=kOutput, calls=%fused_computation.8 | convolution fusion | flops 11284119552 | bytes 26476544 | tf_op jit(solution)/shard_map/dot_general | solution.py:250
  182.1 12.5 %reduce-scatter.2.cloned.1.call-done = bf16[384,2048]{1,0:T(8,128)(2,1)} async-done(((bf16[768,2048]{1,0:T(8,128)(2,1)}), bf16[384,2048]{1,0:T(8,128)(2,1)}) %reduce-scatter.2.cloned.1.call-update) | async-done | bytes 1572880 | tf_op jit(solution)/shard_map/reduce_scatter | solution.py:249
  194.6 6.9 %all-to-all-start.2 = ((bf16[16,24,2048]{2,1,0:T(8,128)(2,1)}), bf16[16,24,2048]{2,1,0:T(8,128)(2,1)S(1)}, u32[]{:S(2)}, u32[]{:S(2)}) async-start(bf16[16,24,2048]{2,1,0:T(8,128)(2,1)} %bitcast.55), calls=%async_computation.3 | async-start | bytes 3145728 | tf_op jit(solution)/shard_map/all_to_all | solution.py:255
  201.8 34.0 %all-to-all-done.2 = bf16[16,24,2048]{2,1,0:T(8,128)(2,1)S(1)} async-done(((bf16[16,24,2048]{2,1,0:T(8,128)(2,1)}), bf16[16,24,2048]{2,1,0:T(8,128)(2,1)S(1)}, u32[]{:S(2)}, u32[]{:S(2)}) %all-to-all-start.2) | async-done | bytes 1572896 | tf_op jit(solution)/shard_map/all_to_all | solution.py:255
  235.8 2.3 gather_fusion
  238.1 2.4 reshape.194
  240.5 3.3 %multiply_reduce_fusion = f32[128,2048]{1,0:T(8,128)S(1)} fusion(f32[128,2,2048]{2,1,0:T(2,128)S(1)} %reshape.194, f32[128,2]{1,0:T(8,128)S(1)} %copy.31), kind=kLoop, calls=%fused_computation.11 | loop fusion | flops 786432 | bytes 3146752 | tf_op jit(solution)/shard_map/reduce_sum | solution.py:264
  244.0 1.0 fusion.19
  (42 shorter events, 1.7 us)
Async XLA Ops:
  6.5 74.6 %all-gather.3.cloned.1.call-start = ((), (), s32[]{:S(2)}) async-start(), calls=%async_computation.4 | async-start | bytes 6291456 | tf_op jit(solution)/shard_map/all_gather | solution.py:218
  12.9 66.5 %copy-start.4 = (s32[128,2]{0,1:T(2,128)S(1)}, s32[128,2]{0,1:T(2,128)}, u32[]{:S(2)}) copy-start(s32[128,2]{0,1:T(2,128)} %param.28) | copy-start | bytes 3076
  74.0 10.1 %copy-start = (bf16[128,2048]{1,0:T(8,128)(2,1)S(1)}, bf16[128,2048]{1,0:T(8,128)(2,1)}, u32[]{:S(2)}) copy-start(bf16[128,2048]{1,0:T(8,128)(2,1)} %param.20) | copy-start | bytes 1572868
  74.0 10.1 %copy-start.1 = (f32[2048]{0:T(1024)S(1)}, f32[2048]{0:T(1024)}, u32[]{:S(2)}) copy-start(f32[2048]{0:T(1024)} %param.22) | copy-start | bytes 24580
  75.9 5.2 %all-to-all-start = ((bf16[2,128,512]{1,2,0:T(8,128)(2,1)}), bf16[2,128,512]{1,2,0:T(8,128)(2,1)S(1)}, u32[]{:S(2)}, u32[]{:S(2)}) async-start(bf16[2,128,512]{1,2,0:T(8,128)(2,1)} %copy.30), calls=%async_computation | async-start | bytes 524288 | tf_op jit(solution)/shard_map/all_to_all | solution.py:215
  79.3 5.2 %copy-start.2 = (f32[2048]{0:T(1024)S(1)}, f32[2048]{0:T(1024)}, u32[]{:S(2)}) copy-start(f32[2048]{0:T(1024)} %param.23) | copy-start | bytes 24580
  79.3 70.6 %all-gather.5.cloned.1.call-start = ((), (), s32[]{:S(2)}) async-start(), calls=%async_computation.5 | async-start | bytes 4718592 | tf_op jit(solution)/shard_map/all_gather | solution.py:245
  139.1 55.5 %reduce-scatter.2.cloned.1.call-start = ((), (), s32[]{:S(2)}) async-start(), calls=%async_computation.6 | async-start | bytes 4718592 | tf_op jit(solution)/shard_map/reduce_scatter | solution.py:249
  182.1 19.6 %copy-start.5 = (f32[128,2]{0,1:T(2,128)S(1)}, f32[128,2]{0,1:T(2,128)}, u32[]{:S(2)}) copy-start(f32[128,2]{0,1:T(2,128)} %param.29) | copy-start | bytes 3076
  194.6 41.1 %all-to-all-start.2 = ((bf16[16,24,2048]{2,1,0:T(8,128)(2,1)}), bf16[16,24,2048]{2,1,0:T(8,128)(2,1)S(1)}, u32[]{:S(2)}, u32[]{:S(2)}) async-start(bf16[16,24,2048]{2,1,0:T(8,128)(2,1)} %bitcast.55), calls=%async_computation.3 | async-start | bytes 3145728 | tf_op jit(solution)/shard_map/all_to_all | solution.py:255
  238.1 5.8 %copy-start.3 = (f32[2048]{0:T(1024)S(1)}, f32[2048]{0:T(1024)}, u32[]{:S(2)}) copy-start(f32[2048]{0:T(1024)} %param.24) | copy-start | bytes 24580
Sparse Core Ops, SparseCore 0:
  8.9 16.3 all-gather.2
  139.2 10.6 all-gather.4
  182.2 12.3 reduce-scatter.1
